TPU v7x, 32 devices: a whole 2x2x4 slice. The times are simulated.
32 devices in a mesh: sp: 16 (over z, y, x), tp: 2 (over core).
Axes of the slice: x: 2, y: 2, z: 4, core: 2. Of those that a mesh axis runs over, the one named last changes fastest.
Arguments:
- skip_stream_entering: bfloat16 [1024, 2048], P('sp'), may hold values from -6 to 6
- reading_vectors: bfloat16 [1024, 1024], P('sp', 'tp'), may hold values from -6 to 6
- blender_lookup_labels: bfloat16 [1024, 1024], P('sp', 'tp'), may hold values from -6 to 6
- blender_payloads: bfloat16 [1024, 1024], P('sp', 'tp'), may hold values from -6 to 6
- blender_result_valve: bfloat16 [1024, 1024], P('sp', 'tp'), may hold values from -6 to 6
- fading_logits: bfloat16 [2, 1024, 1024], P(None, 'sp', 'tp'), as said below
- amend_speed_logits: bfloat16 [2, 1024, 1024], P(None, 'sp', 'tp'), as said below
- extra_log_fades: float32 [2, 16, 1024], P(None, 'tp', 'sp'), may hold values from -3 to 0
- present_reward_factors: float32 [1024], P('tp'), may hold values from -1.2 to 1.2
- attender_scaling_vector: float32 [1024], P('tp'), may hold values from 0.1 to 1.9
- blender_result_projector: bfloat16 [1024, 2048], P('tp'), may hold values from -0.1875 to 0.1875
- blender_scaling_vector: float32 [2048], replicated, may hold values from 0.1 to 1.9
- perceptron_valve_factors: bfloat16 [2048, 5632], P('sp', 'tp'), may hold values from -0.125 to 0.125
- perceptron_widen_factors: bfloat16 [2048, 5632], P('sp', 'tp'), may hold values from -0.125 to 0.125
- perceptron_shrink_factors: bfloat16 [5632, 2048], P('tp', 'sp'), may hold values from -0.078125 to 0.078125
- closing_scaling_vector: float32 [2048], replicated, may hold values from 0.1 to 1.9
Outputs:
- result: bfloat16 [1024, 2048], P(('sp', 'tp'))
Inputs may be any that keep to these rules, and one draw needn't show every extreme that they name: `fading_logits`: decay pre-activations. `amend_speed_logits`: correction-rate pre-activations.
All inputs are finite; a program needn't handle non-finite values.
Results may differ from a plain program's by a relative error of at most 0.02.
Values may be sent and summed in bfloat16 or wider, within the bound.
A program may use at most 128 MiB of HBM per device.

v0:
```python
import jax
import jax.numpy as jnp
from jax import lax
from jax.sharding import PartitionSpec as P

RESIDUAL_SCALE = 2.0**0.25
NORM_EPS = 1e-05
GROUP_EPS = 0.00064
KEY_EPS = 1e-06
PRECISE = lax.Precision.HIGHEST


def carried_in(value, axis, join, neutral, backward):
    count = lax.axis_size(axis)
    place = lax.axis_index(axis)
    ahead = count - 1 - place if backward else place
    gathered = jax.tree.map(
        lambda a, kind: lax.all_gather(a.astype(kind), axis), value, (jnp.bfloat16, jnp.bfloat16)
    )
    state = jax.tree.map(lambda a, e: jnp.zeros_like(a) + jnp.asarray(e, a.dtype), value, neutral)

    def one(step, state):
        source = count - 1 - step if backward else step
        return join(
            state,
            jax.tree.map(
                lambda a, own: lax.dynamic_index_in_dim(a, source, 0, False).astype(own.dtype),
                gathered,
                value,
            ),
        )

    return lax.fori_loop(0, ahead, one, state)


def layer_norm(summand, gain_vec):
    center = jnp.mean(summand, -1, keepdims=True)
    spread = jnp.mean(jnp.square(summand - center), -1, keepdims=True)
    return (summand - center) * lax.rsqrt(spread + NORM_EPS) * gain_vec


def chain_blocks(earlier, later):
    return (
        jnp.einsum("hij,hjk->hik", earlier[0], later[0], precision=PRECISE),
        jnp.einsum("hij,hjk->hik", earlier[1], later[0], precision=PRECISE) + later[1],
    )


def advance(joined, inputs):
    query_vec, decay_vec, write_key, padded_value, erase_vec, refill_vec = inputs
    erased = jnp.einsum("hji,hj->hi", joined, erase_vec, precision=PRECISE)
    joined = (
        joined * decay_vec[:, :, None]
        + refill_vec[:, :, None] * erased[:, None, :]
        + write_key[:, :, None] * padded_value[:, None, :]
    )
    return (joined, jnp.einsum("hji,hj->hi", joined, query_vec, precision=PRECISE))


def shards(
    skip_stream_entering,
    reading_vectors,
    blender_lookup_labels,
    blender_payloads,
    blender_result_valve,
    fading_logits,
    amend_speed_logits,
    extra_log_fades,
    present_reward_factors,
    attender_scaling_vector,
    blender_result_projector,
    blender_scaling_vector,
    perceptron_valve_factors,
    perceptron_widen_factors,
    perceptron_shrink_factors,
    closing_scaling_vector,
):
    tok_rows = reading_vectors.shape[0]
    local_attender_number = extra_log_fades.shape[1]
    head_size = reading_vectors.shape[1] // local_attender_number
    row_share = tok_rows // lax.axis_size("tp")
    row_start = lax.axis_index("tp") * row_share

    def split_attenders(tensor):
        return tensor.reshape(tensor.shape[:-1] + (local_attender_number, head_size))

    def both_ways(forward_part, backward_part):
        return jnp.concatenate([forward_part, jnp.flip(backward_part, 0)], axis=1)

    entire_asking_lines = split_attenders(reading_vectors.astype(jnp.float32))
    key_rows = split_attenders(blender_lookup_labels.astype(jnp.float32))
    payload_line_slab = split_attenders(blender_payloads.astype(jnp.float32))
    key_square = jnp.sum(key_rows * key_rows, -1, keepdims=True)
    unit_keys = key_rows * lax.rsqrt(key_square + KEY_EPS)
    fading_log_amount = (
        split_attenders(-jnp.exp(-jax.nn.softplus(-fading_logits.astype(jnp.float32)) - 0.5))
        + jnp.swapaxes(extra_log_fades, 1, 2)[..., None]
    )
    decays = jnp.exp(fading_log_amount)
    icl_rates = split_attenders(jax.nn.sigmoid(amend_speed_logits.astype(jnp.float32)))
    stored_label_lines = key_rows[None] * icl_rates
    refills = unit_keys[None] * icl_rates
    padded_payload = jnp.concatenate(
        [payload_line_slab, jnp.zeros_like(payload_line_slab)], axis=-1
    )
    sequence_in = (
        both_ways(entire_asking_lines, entire_asking_lines),
        both_ways(decays[0], decays[1]),
        both_ways(stored_label_lines[0], stored_label_lines[1]),
        both_ways(padded_payload, padded_payload),
        both_ways(-unit_keys, -unit_keys),
        both_ways(refills[0], refills[1]),
    )
    identity = jnp.broadcast_to(
        jnp.eye(head_size, dtype=jnp.float32), (2 * local_attender_number, head_size, head_size)
    )
    start_joined = jnp.concatenate([jnp.zeros_like(identity), identity], axis=-1)
    joined_end, readings = lax.scan(advance, start_joined, sequence_in, unroll=16)
    state_end = jnp.swapaxes(joined_end[..., :head_size], 1, 2)
    prod_end = jnp.swapaxes(joined_end[..., head_size:], 1, 2)
    local_out = readings[..., :head_size]
    carried_dir = readings[..., head_size:]
    neutral = (identity[:local_attender_number], jnp.zeros_like(identity[:local_attender_number]))
    enter_fwd = carried_in(
        (prod_end[:local_attender_number], state_end[:local_attender_number]),
        "sp",
        chain_blocks,
        neutral,
        False,
    )[1]
    enter_bwd = carried_in(
        (prod_end[local_attender_number:], state_end[local_attender_number:]),
        "sp",
        chain_blocks,
        neutral,
        True,
    )[1]
    entering = jnp.concatenate([enter_fwd, enter_bwd], axis=0)
    complete = local_out + jnp.einsum("hij,thj->thi", entering, carried_dir, precision=PRECISE)
    summed = complete[:, :local_attender_number] + jnp.flip(complete[:, local_attender_number:], 0)
    center = jnp.mean(summed, -1, keepdims=True)
    spread = jnp.mean(jnp.square(summed - center), -1, keepdims=True)
    rescaled_lines = (
        (summed - center) * lax.rsqrt(spread + GROUP_EPS) * split_attenders(attender_scaling_vector)
    )
    present_reward_summand = (
        jnp.sum(
            entire_asking_lines
            * (stored_label_lines[0] + stored_label_lines[1])
            * split_attenders(present_reward_factors),
            -1,
            keepdims=True,
        )
        * payload_line_slab
    )
    merged_attender_lines = (
        (rescaled_lines + present_reward_summand)
        * split_attenders(blender_result_valve.astype(jnp.float32))
    ).reshape(tok_rows, -1)
    merged_attender_lines = merged_attender_lines.astype(jnp.bfloat16)
    mixsum = lax.psum_scatter(
        jnp.dot(
            merged_attender_lines, blender_result_projector, preferred_element_type=jnp.float32
        ).astype(jnp.bfloat16),
        "tp",
        scatter_dimension=0,
        tiled=True,
    ).astype(jnp.float32)
    residual = lax.dynamic_slice_in_dim(skip_stream_entering, row_start, row_share, 0).astype(
        jnp.float32
    )
    middle = layer_norm(RESIDUAL_SCALE * residual + mixsum, blender_scaling_vector).astype(
        jnp.bfloat16
    )
    all_middle = lax.all_gather(middle, "tp", axis=0, tiled=True)
    gate_pre = jnp.dot(
        all_middle,
        lax.all_gather(perceptron_valve_factors, "sp", axis=0, tiled=True),
        preferred_element_type=jnp.float32,
    )
    up_pre = jnp.dot(
        all_middle,
        lax.all_gather(perceptron_widen_factors, "sp", axis=0, tiled=True),
        preferred_element_type=jnp.float32,
    )
    inner_act = (jax.nn.silu(gate_pre) * up_pre).astype(jnp.bfloat16)
    down_terms = jnp.dot(
        inner_act,
        lax.all_gather(perceptron_shrink_factors, "sp", axis=1, tiled=True),
        preferred_element_type=jnp.float32,
    )
    downsum = lax.psum_scatter(
        down_terms.astype(jnp.bfloat16), "tp", scatter_dimension=0, tiled=True
    ).astype(jnp.float32)
    return layer_norm(
        RESIDUAL_SCALE * middle.astype(jnp.float32) + downsum, closing_scaling_vector
    ).astype(jnp.bfloat16)


def solution(mesh):
    return jax.shard_map(
        shards,
        mesh=mesh,
        in_specs=(
            P("sp", None),
            P("sp", "tp"),
            P("sp", "tp"),
            P("sp", "tp"),
            P("sp", "tp"),
            P(None, "sp", "tp"),
            P(None, "sp", "tp"),
            P(None, "tp", "sp"),
            P("tp"),
            P("tp"),
            P("tp", None),
            P(),
            P("sp", "tp"),
            P("sp", "tp"),
            P("tp", "sp"),
            P(),
        ),
        out_specs=P(("sp", "tp"), None),
        check_vma=False,
    )
```

profile of v0, /device:TPU:0, one launch (start us, length us, event | category | flops | bytes accessed | tf_op | source)
XLA Modules:
  0.0 1114.9 jit_solution(17199332043154124790)
XLA Ops:
  31.3 287.5 %while.38 = (s32[]{:T(128)}, f32[16,64,128]{2,1,0:T(8,128)S(1)}, f32[4,16,16,128]{3,1,0,2:T(8,128)}, f32[4,16,16,64]{3,2,1,0:T(8,128)}, f32[4,16,16,64]{3,2,1,0:...) while((s32[]{:T(128)}, f32[16,64,128]{2,1,0:T(8,128)S(1)}, ...), condition=%wide.region_2.3_spmd, body=%wide.region_1.2_spmd.sunk | while | flops 108003344 | bytes 25330840 | solution.py:118
  66.4 3.5 multiply_add_fusion.101
  75.3 5.2 multiply_add_fusion.102
  107.2 6.8 multiply_add_fusion.103
  131.9 3.5 multiply_add_fusion.101
  140.8 5.2 multiply_add_fusion.102
  172.7 6.8 multiply_add_fusion.103
  197.4 3.5 multiply_add_fusion.101
  206.4 5.2 multiply_add_fusion.102
  238.2 6.8 multiply_add_fusion.103
  263.0 3.5 multiply_add_fusion.101
  271.9 5.2 multiply_add_fusion.102
  303.8 6.8 multiply_add_fusion.103
  325.0 59.9 %all-gather.18.cloned.1.call-done = bf16[128,64,64]{2,1,0:T(8,128)(2,1)} async-done(((bf16[8,64,64]{2,1,0:T(8,128)(2,1)}), bf16[128,64,64]{2,1,0:T(8,128)(2,1)}) %all-gather.18.cloned.1.call-update) | async-done | bytes 1048592 | tf_op jit(solution)/shard_map/all_gather | solution.py:18
  384.9 62.0 %all-gather.20.cloned.1.call-done = bf16[128,64,64]{2,1,0:T(8,128)(2,1)} async-done(((bf16[8,64,64]{2,1,0:T(8,128)(2,1)}), bf16[128,64,64]{2,1,0:T(8,128)(2,1)}) %all-gather.20.cloned.1.call-update) | async-done | bytes 1048592 | tf_op jit(solution)/shard_map/all_gather | solution.py:18
  447.1 61.9 %all-gather.22.cloned.1.call-done = bf16[128,64,64]{2,1,0:T(8,128)(2,1)} async-done(((bf16[8,64,64]{2,1,0:T(8,128)(2,1)}), bf16[128,64,64]{2,1,0:T(8,128)(2,1)}) %all-gather.22.cloned.1.call-update) | async-done | bytes 1048592 | tf_op jit(solution)/shard_map/all_gather | solution.py:18
  508.9 61.8 %all-gather.24.cloned.1.call-done = bf16[128,64,64]{2,1,0:T(8,128)(2,1)} async-done(((bf16[8,64,64]{2,1,0:T(8,128)(2,1)}), bf16[128,64,64]{2,1,0:T(8,128)(2,1)}) %all-gather.24.cloned.1.call-update) | async-done | bytes 1048592 | tf_op jit(solution)/shard_map/all_gather | solution.py:18
  570.8 35.0 %while.40 = (s32[]{:T(128)}, f32[8,64,64]{1,2,0:T(8,128)S(1)}, s32[]{:T(128)}, bf16[16,8,64,64]{3,2,1,0:T(8,128)(2,1)}, bf16[16,8,64,64]{3,2,1,0:T(8,128)(2,1)},...) while((s32[]{:T(128)}, f32[8,64,64]{1,2,0:T(8,128)S(1)}, s32[]{:T(128)}, ...), condition=%wide.region_6.7_spmd, body=%wide.region_5.6_spmd.sunk | while | flops 25231364 | bytes 983187 | solution.py:33
  620.4 140.0 %all-gather.12.cloned.1.call-done = bf16[2048,2816]{1,0:T(8,128)(2,1)} async-done(((bf16[128,2816]{1,0:T(8,128)(2,1)}), bf16[2048,2816]{1,0:T(8,128)(2,1)}) %all-gather.12.cloned.1.call-update) | async-done | bytes 11534352 | tf_op jit(solution)/shard_map/all_gather | solution.py:178
  760.4 6.4 fusion.134
  766.8 136.0 %all-gather.14.cloned.1.call-done = bf16[2048,2816]{1,0:T(8,128)(2,1)} async-done(((bf16[128,2816]{1,0:T(8,128)(2,1)}), bf16[2048,2816]{1,0:T(8,128)(2,1)}) %all-gather.14.cloned.1.call-update) | async-done | bytes 11534352 | tf_op jit(solution)/shard_map/all_gather | solution.py:183
  902.8 183.0 %all-gather.16.cloned.1.call-done = bf16[2816,2048]{1,0:T(8,128)(2,1)} async-done(((bf16[2816,128]{1,0:T(8,128)(2,1)}), bf16[2816,2048]{1,0:T(8,128)(2,1)}) %all-gather.16.cloned.1.call-update) | async-done | bytes 11534352 | tf_op jit(solution)/shard_map/all_gather | solution.py:189
  1085.8 12.4 %convolution_convert_fusion = bf16[64,2048]{1,0:T(8,128)(2,1)} fusion(bf16[2816,2048]{1,0:T(8,128)(2,1)} %all-gather.16.cloned.1.call-done, bf16[64,2048]{1,0:T(8,128)(2,1)S(1)} %all_gather.44, bf16[2048,2816]{1,0:T(8,128)(2,1)} %all-gather.14.cloned.1.call-done, f32[64,2816]{1,0:T(8,128)S(1)} %fusion.134), kind=kOutput, calls=%fused_computation.231 | convolution fusion | flops 1477607424 | bytes 24313856 | tf_op jit(solution)/shard_map/dot_general | solution.py:187
  1098.2 6.1 reduce-scatter.5.cloned.1.call-done
  (401 shorter events, 282.8 us)
Async XLA Ops:
  6.5 603.7 %copy-start = (bf16[512,2048]{1,0:T(8,128)(2,1)S(1)}, bf16[512,2048]{1,0:T(8,128)(2,1)}, u32[]{:S(2)}) copy-start(bf16[512,2048]{1,0:T(8,128)(2,1)} %param.32) | copy-start | bytes 6291460
  6.5 4.9 copy-start.11
  6.5 378.4 %all-gather.18.cloned.1.call-start = ((), (), s32[]{:S(2)}) async-start(), calls=%async_computation.7 | async-start | bytes 2228224 | tf_op jit(solution)/shard_map/all_gather | solution.py:18
  7.7 15.0 %copy-start.1 = (f32[64,8,64]{2,1,0:T(8,128)}, f32[64,8,64]{2,1,0:T(8,128)S(1)}, u32[]{:S(2)}) copy-start(f32[64,8,64]{2,1,0:T(8,128)S(1)} %reshape.385) | copy-start | bytes 393220
  14.5 5.4 copy-start.14
  18.9 4.5 copy-start.12
  22.7 5.5 copy-start.5
  23.6 6.4 copy-start.3
  26.2 4.0 copy-start.9
  318.8 5.0 copy-start.17
  318.8 5.1 copy-start.2
  318.8 5.3 copy-start.13
  319.8 5.1 copy-start.18
  321.7 125.2 %all-gather.20.cloned.1.call-start = ((), (), s32[]{:S(2)}) async-start(), calls=%async_computation.8 | async-start | bytes 2228224 | tf_op jit(solution)/shard_map/all_gather | solution.py:18
  322.4 186.5 %all-gather.22.cloned.1.call-start = ((), (), s32[]{:S(2)}) async-start(), calls=%async_computation.9 | async-start | bytes 2228224 | tf_op jit(solution)/shard_map/all_gather | solution.py:18
  323.2 247.6 %all-gather.24.cloned.1.call-start = ((), (), s32[]{:S(2)}) async-start(), calls=%async_computation.10 | async-start | bytes 2228224 | tf_op jit(solution)/shard_map/all_gather | solution.py:18
  323.8 291.5 %reduce-scatter.3.cloned.1.call-start = ((), (), s32[]{:S(2)}) async-start(), calls=%async_computation.2 | async-start | bytes 393216 | tf_op jit(solution)/shard_map/reduce_scatter | solution.py:161
  610.3 5.0 copy-start.10
  610.3 7.2 copy-start.15
  611.5 148.9 %all-gather.12.cloned.1.call-start = ((), (), s32[]{:S(2)}) async-start(), calls=%async_computation.3 | async-start | bytes 12255232 | tf_op jit(solution)/shard_map/all_gather | solution.py:178
  612.1 290.8 %all-gather.14.cloned.1.call-start = ((), (), s32[]{:S(2)}) async-start(), calls=%async_computation.4 | async-start | bytes 12255232 | tf_op jit(solution)/shard_map/all_gather | solution.py:183
  612.8 473.0 %all-gather.16.cloned.1.call-start = ((), (), s32[]{:S(2)}) async-start(), calls=%async_computation.5 | async-start | bytes 12255232 | tf_op jit(solution)/shard_map/all_gather | solution.py:189
  613.6 490.7 %reduce-scatter.5.cloned.1.call-start = ((), (), s32[]{:S(2)}) async-start(), calls=%async_computation.6 | async-start | bytes 393216 | tf_op jit(solution)/shard_map/reduce_scatter | solution.py:192
  766.8 339.7 %copy-start.16 = (f32[2048]{0:T(1024)S(1)}, f32[2048]{0:T(1024)}, u32[]{:S(2)}) copy-start(f32[2048]{0:T(1024)} %param.37) | copy-start | bytes 24580
  (4 other events, 15.0 us)
Sparse Core Ops, SparseCore 0:
  321.8 63.0 all-gather.17
  387.7 59.1 all-gather.19
  449.7 59.2 all-gather.21
  511.6 59.1 all-gather.23
  611.6 3.5 reduce-scatter.2
  617.8 142.5 all-gather.11
  763.2 139.5 all-gather.13
  905.5 180.2 all-gather.15
  1098.3 5.9 reduce-scatter.4
where the time goes:
time: 1120 us; the launch traced here: 1110 us
  waiting for transfers between devices  715 us (64%)
  matrix products  213 us (19%)
  other arithmetic  90.2 us (8%)
  local copies, waits for them, and re-layouts  52.8 us (5%)
  loops' own time  27 us (2%)
  between operations  13.8 us (1%)
    all_gather x4, waiting for transfers between devices, carried_in(): lax.all_gather(a.astype(kind), axis)  246 us
    all_gather x1, waiting for transfers between devices, shards(): lax.all_gather(perceptron_shrink_factors, 'sp', axis=1, tiled=True)  183 us
    all_gather x1, waiting for transfers between devices, shards(): lax.all_gather(perceptron_valve_factors, 'sp', axis=0, tiled=True)  140 us
    all_gather x1, waiting for transfers between devices, shards(): lax.all_gather(perceptron_widen_factors, 'sp', axis=0, tiled=True)  136 us
    dot_general x64, matrix products, advance(): jnp.einsum('hji,hj->hi', joined, query_vec, precision=PRECISE)  86.5 us
    dot_general x64, matrix products, advance(): erased = jnp.einsum('hji,hj->hi', joined, erase_vec, precision=PRECISE)  86.3 us
    add x16, other arithmetic, advance(): joined * decay_vec[:, :, None] + refill_vec[:, :, None] * erased[:, None, :]  69.3 us
    another operation x1, loops' own time, shards(): lax.scan(advance, start_joined, sequence_in, unroll=16)  26.2 us
  transfers between devices with their start and end apart: 9, of which 9 were waited for; matrix products, arithmetic and copies ran while one was open for 1% of the time, Pallas kernels for 0%

commit v1 on v0

v1 whole, which is shorter than its diff:
```python
import functools
import jax
import jax.numpy as jnp
from jax import lax
from jax.experimental import pallas as pl
from jax.experimental.pallas import tpu as pltpu
from jax.sharding import PartitionSpec as P

RESIDUAL_SCALE = 2.0**0.25
NORM_EPS = 1e-05
GROUP_EPS = 0.00064
KEY_EPS = 1e-06
MESH = pl.DeviceIdType.MESH
VMEM = pl.BlockSpec(memory_space=pltpu.VMEM)
BF = jnp.bfloat16
F32 = jnp.float32


def layer_norm(summand, gain_vec):
    center = jnp.mean(summand, -1, keepdims=True)
    spread = jnp.mean(jnp.square(summand - center), -1, keepdims=True)
    return (summand - center) * lax.rsqrt(spread + NORM_EPS) * gain_vec


def remote(src, dst, send_sem, recv_sem, device):
    return pltpu.make_async_remote_copy(
        src_ref=src,
        dst_ref=dst,
        send_sem=send_sem,
        recv_sem=recv_sem,
        device_id=device,
        device_id_type=MESH,
    )


def greet(devices):
    barrier = pltpu.get_barrier_semaphore()
    for device in devices:
        pl.semaphore_signal(barrier, inc=1, device_id=device, device_id_type=MESH)
    pl.semaphore_wait(barrier, len(devices))


def split_dot(wide, narrow):
    high = wide.astype(BF)
    low = (wide - high.astype(F32)).astype(BF)
    return jnp.dot(high, narrow, preferred_element_type=F32) + jnp.dot(
        low, narrow, preferred_element_type=F32
    )


def recur_kernel(n, pack, vpad, weights, readings, joined, spread, send, recv):
    me = lax.axis_index("sp")
    peers = [lax.rem(me + k, n) for k in range(1, n)]
    greet([{"sp": p} for p in peers])
    copies = [
        remote(weights.at[p], spread.at[me], send.at[k], recv.at[k], {"sp": p})
        for k, p in enumerate(peers)
    ]
    for copy in copies:
        copy.start()
    spread[me] = weights[me]
    blocks, heads, size, _ = pack.shape
    rows = blocks * 8
    wide = 2 * size
    group = 2 if heads % 2 == 0 else 1
    eye = jnp.where(
        lax.broadcasted_iota(jnp.int32, (size, wide), 0) + size
        == lax.broadcasted_iota(jnp.int32, (size, wide), 1),
        1.0,
        0.0,
    ).astype(F32)

    def head_group(hh, carry):
        def block(tb, states):
            states = list(states)
            for i in range(8):
                t = tb * 8 + i
                for g in range(group):
                    h = hh * group + g
                    for d in range(2):
                        row = t if d == 0 else rows - 1 - t
                        vecs = [
                            jnp.broadcast_to(
                                pack[tb, h, :, pl.ds((d * 4 + c) * 8 + i, 1)], (size, wide)
                            )
                            for c in range(4)
                        ]
                        state = states[g * 2 + d]
                        erased = jnp.sum(state * vecs[1], 0, keepdims=True)
                        state = state * vecs[0] + vecs[2] * (
                            vpad[h, pl.ds(row, 1), :] - erased
                        )
                        readings[d, h, pl.ds(row, 1), :] = jnp.sum(
                            state * vecs[3], 0, keepdims=True
                        )
                        states[g * 2 + d] = state
            return tuple(states)

        states = lax.fori_loop(0, blocks, block, (eye,) * (2 * group))
        for g in range(group):
            for d in range(2):
                joined[d * heads + hh * group + g] = states[g * 2 + d].astype(BF)
        return carry

    lax.fori_loop(0, heads // group, head_group, 0)
    for copy in copies:
        copy.wait()


def chain_kernel(n, joined, entering, held, carried, send, recv, send_back, recv_back):
    me = lax.axis_index("sp")
    peers = [lax.rem(me + k, n) for k in range(1, n)]
    greet([{"sp": p} for p in peers])
    copies = [
        remote(joined.at[p], held.at[me], send.at[k], recv.at[k], {"sp": p})
        for k, p in enumerate(peers)
    ]
    for copy in copies:
        copy.start()
    held[me] = joined[me]
    for copy in copies:
        copy.wait()
    size = entering.shape[1]
    back = me // (n // 2)
    state = jnp.zeros((size, size), F32)
    for step in range(n):
        at = back * (n - 1 - step) + (1 - back) * step
        carried[at] = state.astype(BF)
        if step < n - 1:
            block = held[at]
            high = state.astype(BF)
            low = (state - high.astype(F32)).astype(BF)
            move = block[:, size:]
            state = (
                jnp.dot(move, high, preferred_element_type=F32)
                + jnp.dot(move, low, preferred_element_type=F32)
                + block[:, :size].astype(F32)
            )
    copies = [
        remote(carried.at[p], entering.at[me], send_back.at[k], recv_back.at[k], {"sp": p})
        for k, p in enumerate(peers)
    ]
    for copy in copies:
        copy.start()
    entering[me] = carried[me]
    for copy in copies:
        copy.wait()


def places(n1, n2, n_tp):
    sp, tm = lax.axis_index("sp"), lax.axis_index("tp")
    zm, pm = sp // n2, lax.rem(sp, n2)
    along = [{"sp": lax.rem(zm + k, n1) * n2 + pm} for k in range(1, n1)]
    plane = [{"sp": zm * n2 + lax.rem(pm + m, n2)} for m in range(1, n2)]
    across = [{"tp": lax.rem(tm + t, n_tp)} for t in range(1, n_tp)]
    return tm, zm, pm, along, plane, across


def gather_kernel(
    n1,
    n2,
    n_tp,
    readings,
    entering,
    bonus,
    valve,
    gain,
    proj,
    residual,
    scale,
    gathered,
    middle,
    mixed,
    parts,
    landed,
    send_t,
    recv_t,
    send_z,
    recv_z,
    send_p,
    recv_p,
    send_c,
    recv_c,
):
    tm, zm, pm, along, plane, across = places(n1, n2, n_tp)
    greet(along + plane + across)
    heads = readings.shape[1]
    rows = readings.shape[2]
    size = entering.shape[1]
    for h in range(heads):
        cols = slice(h * size, (h + 1) * size)
        total = None
        for d in range(2):
            read = readings[d, h]
            term = read[:, :size] + split_dot(read[:, size:], entering[d * heads + h])
            total = term if total is None else total + term
        center = jnp.mean(total, -1, keepdims=True)
        spread = jnp.mean(jnp.square(total - center), -1, keepdims=True)
        normed = (total - center) * lax.rsqrt(spread + GROUP_EPS) * gain[:, cols]
        mixed[:, cols] = ((normed + bonus[:, cols]) * valve[:, cols].astype(F32)).astype(BF)
    share = rows // n_tp
    product = jnp.dot(mixed[...], proj[...], preferred_element_type=F32).astype(BF)
    for t in range(n_tp):
        parts[t] = product[t * share : (t + 1) * share]
    copies = [
        remote(
            parts.at[lax.rem(tm + t + 1, n_tp)], landed.at[t], send_t.at[t], recv_t.at[t], dev
        )
        for t, dev in enumerate(across)
    ]
    for copy in copies:
        copy.start()
    for copy in copies:
        copy.wait()
    mixsum = parts[tm].astype(F32)
    for t in range(n_tp - 1):
        mixsum = mixsum + landed[t].astype(F32)
    own = layer_norm(RESIDUAL_SCALE * residual[...].astype(F32) + mixsum, scale[...]).astype(BF)
    middle[...] = own
    gathered[tm, zm, pm] = own

    started = []

    def begin(copy):
        copy.start()
        started.append(copy)
        return copy

    def slot(k, m):
        z, p = lax.rem(zm + n1 - k, n1), lax.rem(pm + n2 - m, n2)
        return gathered.at[tm, z, p]

    first = slot(0, 0)
    zs = [
        begin(remote(first, first, send_z.at[k], recv_z.at[k], dev))
        for k, dev in enumerate(along)
    ]

    def to_plane(k):
        return [
            begin(remote(slot(k, 0), slot(k, 0), send_p.at[k, m], recv_p.at[k, m], dev))
            for m, dev in enumerate(plane)
        ]

    def to_cores(k, m):
        for t, dev in enumerate(across):
            begin(
                remote(slot(k, m), slot(k, m), send_c.at[t, k, m], recv_c.at[t, k, m], dev)
            )

    ps = [to_plane(0)]
    to_cores(0, 0)
    for k in range(1, n1):
        zs[k - 1].wait_recv()
        ps.append(to_plane(k))
        to_cores(k, 0)
    for k in range(n1):
        for m in range(1, n2):
            ps[k][m - 1].wait_recv()
            to_cores(k, m)
    plain = set(map(id, zs)) | {id(c) for row in ps for c in row}
    for copy in started:
        copy.wait_send()
        if id(copy) not in plain:
            copy.wait_recv()


def scatter_kernel(
    n1,
    n2,
    n_tp,
    terms,
    middle,
    scale,
    out,
    land_c,
    plane_sum,
    land_p,
    line_sum,
    land_z,
    send_c,
    recv_c,
    send_p,
    recv_p,
    send_z,
    recv_z,
):
    tm, zm, pm, along, plane, across = places(n1, n2, n_tp)
    greet(along + plane + across)
    order = list(range(1, n1)) + [0]
    started = []

    def begin(copy):
        copy.start()
        started.append(copy)
        return copy

    def line(k):
        return lax.rem(zm + k, n1)

    cores = {
        k: [
            begin(
                remote(
                    terms.at[lax.rem(tm + t + 1, n_tp), line(k)],
                    land_c.at[t, k],
                    send_c.at[t, k],
                    recv_c.at[t, k],
                    dev,
                )
            )
            for t, dev in enumerate(across)
        ]
        for k in order
    }
    planes = {}
    for k in order:
        for copy in cores[k]:
            copy.wait_recv()
        for p in range(n2):
            total = terms[tm, line(k), p].astype(F32)
            for t in range(n_tp - 1):
                total = total + land_c[t, k, p].astype(F32)
            plane_sum[k, p] = total.astype(BF)
        planes[k] = [
            begin(
                remote(
                    plane_sum.at[k, lax.rem(pm + m + 1, n2)],
                    land_p.at[k, m],
                    send_p.at[k, m],
                    recv_p.at[k, m],
                    dev,
                )
            )
            for m, dev in enumerate(plane)
        ]
    lines = []
    for k in order:
        for copy in planes[k]:
            copy.wait_recv()
        total = plane_sum[k, pm].astype(F32)
        for m in range(n2 - 1):
            total = total + land_p[k, m].astype(F32)
        if k:
            line_sum[k - 1] = total.astype(BF)
            lines.append(
                begin(
                    remote(
                        line_sum.at[k - 1],
                        land_z.at[k - 1],
                        send_z.at[k - 1],
                        recv_z.at[k - 1],
                        along[k - 1],
                    )
                )
            )
    for k, copy in enumerate(lines):
        copy.wait_recv()
        total = total + land_z[k].astype(F32)
    out[...] = layer_norm(RESIDUAL_SCALE * middle[...].astype(F32) + total, scale[...]).astype(BF)
    for copy in started:
        copy.wait_send()


def params(number):
    return pltpu.CompilerParams(
        collective_id=number, has_side_effects=True, vmem_limit_bytes=60 * 1024 * 1024
    )


def sds(shape, kind):
    return jax.ShapeDtypeStruct(shape, kind)


def chain_gathered(joined, n, heads, size):
    every = lax.all_gather(joined, "sp")
    me = lax.axis_index("sp")

    def walk(half, ahead, backward):
        def one(step, state):
            block = half[n - 1 - step if backward else step].astype(F32)
            return (
                jnp.einsum(
                    "hij,hjk->hik", block[..., size:], state, precision=lax.Precision.HIGHEST
                )
                + block[..., :size]
            )

        return lax.fori_loop(0, ahead, one, jnp.zeros((heads, size, size), F32))

    return jnp.concatenate(
        [walk(every[:, :heads], me, False), walk(every[:, heads:], n - 1 - me, True)], 0
    ).astype(BF)


def shards(
    skip_stream_entering,
    reading_vectors,
    blender_lookup_labels,
    blender_payloads,
    blender_result_valve,
    fading_logits,
    amend_speed_logits,
    extra_log_fades,
    present_reward_factors,
    attender_scaling_vector,
    blender_result_projector,
    blender_scaling_vector,
    perceptron_valve_factors,
    perceptron_widen_factors,
    perceptron_shrink_factors,
    closing_scaling_vector,
):
    n, n_tp = lax.axis_size("sp"), lax.axis_size("tp")
    n1 = 4 if n % 4 == 0 else 1
    n2 = n // n1
    rows, width = reading_vectors.shape
    heads = extra_log_fades.shape[1]
    size = width // heads
    model = skip_stream_entering.shape[1]
    share = rows // n_tp
    dma = pltpu.SemaphoreType.DMA

    def split(tensor):
        return tensor.reshape(tensor.shape[:-1] + (heads, size))

    query = split(reading_vectors.astype(F32))
    key = split(blender_lookup_labels.astype(F32))
    value = split(blender_payloads.astype(F32))
    erase = key / (jnp.sum(key * key, -1, keepdims=True) + KEY_EPS)
    decays = jnp.exp(
        split(-jnp.exp(-jax.nn.softplus(-fading_logits.astype(F32)) - 0.5))
        + jnp.swapaxes(extra_log_fades, 1, 2)[..., None]
    )
    written = key[None] * split(jax.nn.sigmoid(amend_speed_logits.astype(F32)))
    flip = functools.partial(jnp.flip, axis=0)
    pack = jnp.stack(
        [decays[0], erase, written[0], query]
        + [flip(decays[1]), flip(erase), flip(written[1]), flip(query)]
    )
    pack = pack.reshape(8, rows // 8, 8, heads, size).transpose(1, 3, 4, 0, 2)
    pack = pack.reshape(rows // 8, heads, size, 64)
    vpad = jnp.swapaxes(jnp.concatenate([value, jnp.zeros_like(value)], -1), 0, 1)
    bonus = (
        jnp.sum(query * (written[0] + written[1]) * split(present_reward_factors), -1, keepdims=True)
        * value
    ).reshape(rows, width)

    depth = perceptron_valve_factors.shape[0]
    units = perceptron_valve_factors.shape[1] // n
    weights = jnp.stack(
        [
            perceptron_valve_factors.T.reshape(n, units, depth),
            perceptron_widen_factors.T.reshape(n, units, depth),
            perceptron_shrink_factors.reshape(n, units, depth),
        ],
        1,
    )
    readings, joined, spread = pl.pallas_call(
        functools.partial(recur_kernel, n),
        name="recur",
        out_shape=(
            sds((2, heads, rows, 2 * size), F32),
            sds((2 * heads, size, 2 * size), BF),
            sds(weights.shape, BF),
        ),
        in_specs=[VMEM] * 3,
        out_specs=(VMEM,) * 3,
        scratch_shapes=[dma((n - 1,)), dma((n - 1,))],
        compiler_params=params(0),
    )(pack, vpad, weights)

    if 2 * heads == n:
        entering = pl.pallas_call(
            functools.partial(chain_kernel, n),
            name="chain",
            out_shape=sds((n, size, size), BF),
            in_specs=[VMEM],
            out_specs=VMEM,
            scratch_shapes=[
                pltpu.VMEM((n, size, 2 * size), BF),
                pltpu.VMEM((n, size, size), BF),
            ]
            + [dma((n - 1,))] * 4,
            compiler_params=params(1),
        )(joined)
    else:
        entering = chain_gathered(joined, n, heads, size)

    residual = lax.dynamic_slice_in_dim(
        skip_stream_entering, lax.axis_index("tp") * share, share, 0
    )
    gathered, middle = pl.pallas_call(
        functools.partial(gather_kernel, n1, n2, n_tp),
        name="gather",
        out_shape=(sds((n_tp, n1, n2, share, model), BF), sds((share, model), BF)),
        in_specs=[VMEM] * 8,
        out_specs=(VMEM,) * 2,
        scratch_shapes=[
            pltpu.VMEM((rows, width), BF),
            pltpu.VMEM((n_tp, share, model), BF),
            pltpu.VMEM((n_tp - 1, share, model), BF),
            dma((n_tp - 1,)),
            dma((n_tp - 1,)),
            dma((n1 - 1,)),
            dma((n1 - 1,)),
            dma((n1, n2 - 1)),
            dma((n1, n2 - 1)),
            dma((n_tp - 1, n1, n2)),
            dma((n_tp - 1, n1, n2)),
        ],
        compiler_params=params(2),
    )(
        readings,
        entering,
        bonus,
        blender_result_valve,
        attender_scaling_vector[None],
        blender_result_projector,
        residual,
        blender_scaling_vector[None],
    )

    tokens = gathered.reshape(-1, model)
    gate = spread[:, 0].transpose(0, 2, 1).reshape(model, units)
    up = spread[:, 1].transpose(0, 2, 1).reshape(model, units)
    down = spread[:, 2].transpose(1, 0, 2).reshape(units, model)
    inner = (
        jax.nn.silu(jnp.dot(tokens, gate, preferred_element_type=F32))
        * jnp.dot(tokens, up, preferred_element_type=F32)
    ).astype(BF)
    terms = jnp.dot(inner, down, preferred_element_type=F32).astype(BF)

    return pl.pallas_call(
        functools.partial(scatter_kernel, n1, n2, n_tp),
        name="scatter",
        out_shape=sds((share, model), BF),
        in_specs=[VMEM] * 3,
        out_specs=VMEM,
        scratch_shapes=[
            pltpu.VMEM((n_tp - 1, n1, n2, share, model), BF),
            pltpu.VMEM((n1, n2, share, model), BF),
            pltpu.VMEM((n1, n2 - 1, share, model), BF),
            pltpu.VMEM((n1 - 1, share, model), BF),
            pltpu.VMEM((n1 - 1, share, model), BF),
            dma((n_tp - 1, n1)),
            dma((n_tp - 1, n1)),
            dma((n1, n2 - 1)),
            dma((n1, n2 - 1)),
            dma((n1 - 1,)),
            dma((n1 - 1,)),
        ],
        compiler_params=params(3),
    )(terms.reshape(gathered.shape), middle, closing_scaling_vector[None])


def solution(mesh):
    return jax.shard_map(
        shards,
        mesh=mesh,
        in_specs=(
            P("sp", None),
            P("sp", "tp"),
            P("sp", "tp"),
            P("sp", "tp"),
            P("sp", "tp"),
            P(None, "sp", "tp"),
            P(None, "sp", "tp"),
            P(None, "tp", "sp"),
            P("tp"),
            P("tp"),
            P("tp", None),
            P(),
            P("sp", "tp"),
            P("sp", "tp"),
            P("tp", "sp"),
            P(),
        ),
        out_specs=P(("sp", "tp"), None),
        check_vma=False,
    )
```

time: 1120 us -> 188 us (0.17)
  waiting for transfers between devices: 715 us -> 0 us
  matrix products: 213 us -> 10.6 us
  Pallas kernels: 0 us -> 152 us
  other arithmetic: 90.2 us -> 11.3 us
  local copies, waits for them, and re-layouts: 52.8 us -> 13.4 us
  loops' own time: 27 us -> 0 us
  between operations: 13.8 us -> 0.34 us
    all_gather x7 -> x0, waiting for transfers between devices: 705 us -> none  [the longest x4 246 us: carried_in(): lax.all_gather(a.astype(kind), axis)]
    dot_general x147 -> x2, matrix products: 213 us -> 10.6 us  [the longest x1 6.9 us: shards(): terms = jnp.dot(inner, down, preferred_element_type=F32).astype(BF)]
    pallas_call x0 -> x4, Pallas kernels: none -> 152 us  [the longest x1 55 us: shards(): pl.pallas_call(functools.partial(recur_kernel, n), name='recur', out_shap...]
    add x16 -> x1, other arithmetic: 69.3 us -> 0.62 us  [shards(): erase = key / (jnp.sum(key * key, -1, keepdims=True) + KEY_EPS)]
    another operation x3 -> x0, loops' own time: 27 us -> none  [the longest x1 26.2 us: shards(): lax.scan(advance, start_joined, sequence_in, unroll=16)]
    dynamic_slice x30 -> x1, local copies, waits for them, and re-layouts: 15.7 us -> 0.67 us  [shards(): lax.dynamic_slice_in_dim(skip_stream_entering, lax.axis_index('tp') * sha...]
    mul x15 -> x2, local copies, waits for them, and re-layouts: 13.1 us -> 0.93 us  [the longest x1 0.81 us: shards(): query * (written[0] + written[1]) * split(present_reward_factors)]
  transfers between devices with their start and end apart: 9 -> 0, of which waited for: 9 -> 0; matrix products, arithmetic and copies ran while one was open for 1% -> 0% of each run, Pallas kernels for 0% -> 0%
where the time goes in v1:
time: 188 us; the launch traced here: 187 us
  Pallas kernels  152 us (81%)
  local copies, waits for them, and re-layouts  13.4 us (7%)
  other arithmetic  11.3 us (6%)
  matrix products  10.6 us (6%)
    pallas_call x1, Pallas kernels, shards(): pl.pallas_call(functools.partial(recur_kernel, n), name='recur', out_shap...  55 us
    pallas_call x1, Pallas kernels, shards(): pl.pallas_call(functools.partial(gather_kernel, n1, n2, n_tp), name='gath...  35.9 us
    pallas_call x1, Pallas kernels, shards(): pl.pallas_call(functools.partial(scatter_kernel, n1, n2, n_tp), name='sca...  34.1 us
    pallas_call x1, Pallas kernels, shards(): pl.pallas_call(functools.partial(chain_kernel, n), name='chain', out_shap...  26.9 us
    mul x2, other arithmetic, shards(): jnp.sum(query * (written[0] + written[1]) * split(present_reward_factors)...  6.93 us
    dot_general x1, matrix products, shards(): terms = jnp.dot(inner, down, preferred_element_type=F32).astype(BF)  6.9 us

profile of v1, /device:TPU:0, one launch (start us, length us, event | category | flops | bytes accessed | tf_op | source)
XLA Modules:
  0.0 187.5 jit_solution(16688850107999592771)
XLA Ops:
  0.0 0.8 mul.49
  0.8 0.8 copy.34
  1.6 0.7 constant_dynamic-slice_fusion.residual
  2.3 1.0 reshape.77
  3.4 0.6 broadcast_add_fusion
  4.4 0.2 fusion.20
  5.0 0.2 copy-done.8
  5.5 5.4 %fusion = f32[64,8,64]{2,1,0:T(8,128)S(1)} fusion(f32[64,8,64]{2,1,0:T(8,128)S(1)} %reshape.79, f32[8,64]{1,0:T(8,128)S(1)} %mul.49, f32[2,64,8,64]{3,2,1,0:T(8,128)S(1)} %broadcast_multiply_fusion), kind=kOutput, calls=%fused_computation | output fusion | flops 98879 | bytes 526336 | tf_op jit(solution)/shard_map/mul | solution.py:445
  11.0 1.6 convert_multiply_fusion.bonus
  12.6 0.7 slice_bitcast_fusion.3
  13.8 0.7 pad_bitcast_fusion.vpad
  14.5 0.3 copy.39
  14.9 1.5 copy.40
  16.4 2.7 %pad_maximum_fusion.weights = bf16[16,3,176,128]{3,2,1,0:T(8,128)(2,1)} fusion(bf16[16,1,176,128]{3,2,1,0:T(8,128)(2,1)} %bitcast.79, bf16[16,1,176,128]{3,2,1,0:T(8,128)(2,1)S(1)} %bitcast.69, bf16[16,1,176,128]{3,2,1,0:T(8,128)(2,1)S(1)} %bitcast.68), kind=kLoop, calls=%fused_computation.2 | loop fusion | flops 2162688 | bytes 4325376 | tf_op jit(solution)/shard_map/stack | solution.py:451
  19.5 0.4 copy.63
  19.8 1.9 copy.41.pack
  21.7 55.0 %recur.1 = (f32[2,8,64,128]{3,2,1,0:T(8,128)}, bf16[16,64,128]{2,1,0:T(8,128)(2,1)}, bf16[16,3,176,128]{3,2,1,0:T(8,128)(2,1)}) custom-call(f32[8,8,64,64]{3,2,1,0:T(8,128)} %copy.41.pack, f32[8,64,128]{2,1,0:T(8,128)} %pad_bitcast_fusion.vpad, bf16[16,3,176,128]{3,2,1,0:T(8,128)(2,1)} %pad_maximum_fusion.weights), custom_call_target="tpu_custom_call" | custom-call | tf_op jit(solution)/shard_map/recur/pallas_call | solution.py:459
  76.7 26.9 %chain.1.entering = bf16[16,64,64]{2,1,0:T(8,128)(2,1)} custom-call(bf16[16,64,128]{2,1,0:T(8,128)(2,1)} %get-tuple-element.11.joined), custom_call_target="tpu_custom_call" | custom-call | tf_op jit(solution)/shard_map/chain/pallas_call | solution.py:474
  103.6 1.7 slice_bitcast_fusion.2
  105.3 35.9 %gather.1 = (bf16[2,4,4,32,2048]{4,3,2,1,0:T(8,128)(2,1)}, bf16[32,2048]{1,0:T(8,128)(2,1)}) custom-call(f32[2,8,64,128]{3,2,1,0:T(8,128)} %get-tuple-element.10.readings, bf16[16,64,64]{2,1,0:T(8,128)(2,1)} %chain.1.entering, f32[64,512]{1,0:T(8,128)} %convert_multiply_fusion.bonus, bf16[64,512]{1,0:T(8,128)(2,1)} %valve.1, f32[1,512]{1,0:T(1,128)} %bitcast.83, ...), custom_call_target="tpu_custom_call" | custom-call | tf_op jit(solution)/shard_map/gather/pallas_call | solution.py:493
  141.2 3.7 %fusion.8 = f32[1024,176]{0,1:T(8,128)S(1)} fusion(bf16[1024,2048]{1,0:T(8,128)(2,1)} %bitcast.84, bf16[16,22,8,128]{3,2,1,0:T(8,128)(2,1)S(1)} %get-tuple-element.15), kind=kOutput, calls=%fused_computation.11 | convolution fusion | flops 738197504 | bytes 5636096 | tf_op jit(solution)/shard_map/dot_general | solution.py:529
  144.9 6.9 %convolution_convert_fusion = bf16[1024,2048]{1,0:T(8,128)(2,1)} fusion(bf16[1024,2048]{1,0:T(8,128)(2,1)} %bitcast.85, bf16[16,22,8,128]{3,2,1,0:T(8,128)(2,1)S(1)} %get-tuple-element.16, bf16[16,22,8,128]{3,2,1,0:T(8,128)(2,1)S(1)} %get-tuple-element.17, f32[1024,176]{0,1:T(8,128)S(1)} %fusion.8), kind=kOutput, calls=%fused_computation.1 | convolution fusion | flops 1479573504 | bytes 10551296 | tf_op jit(solution)/shard_map/dot_general | solution.py:532
  151.8 34.1 %scatter.1 = bf16[32,2048]{1,0:T(8,128)(2,1)} custom-call(bf16[2,4,4,32,2048]{4,3,2,1,0:T(8,128)(2,1)} %bitcast.67, bf16[32,2048]{1,0:T(8,128)(2,1)} %get-tuple-element.14.middle, f32[1,2048]{1,0:T(1,128)} %bitcast.81), custom_call_target="tpu_custom_call" | custom-call | tf_op jit(solution)/shard_map/scatter/pallas_call | solution.py:534
  185.9 1.6 copy.72
  (45 shorter events, 1.9 us)
Async XLA Ops:
  0.0 1.6 copy-start
  0.0 4.2 %copy-start.3 = (bf16[64,512]{1,0:T(8,128)(2,1)S(1)}, bf16[64,512]{1,0:T(8,128)(2,1)}, u32[]{:S(2)}) copy-start(bf16[64,512]{1,0:T(8,128)(2,1)} %param.17) | copy-start | bytes 196612
  0.0 4.4 %copy-start.7 = (bf16[2,64,512]{2,1,0:T(8,128)(2,1)S(1)}, bf16[2,64,512]{2,1,0:T(8,128)(2,1)}, u32[]{:S(2)}) copy-start(bf16[2,64,512]{2,1,0:T(8,128)(2,1)} %param.21) | copy-start | bytes 393220
  4.3 0.9 copy-start.8
  5.5 7.9 %copy-start.4 = (bf16[64,512]{1,0:T(8,128)(2,1)S(1)}, bf16[64,512]{1,0:T(8,128)(2,1)}, u32[]{:S(2)}) copy-start(bf16[64,512]{1,0:T(8,128)(2,1)} %param.17) | copy-start | bytes 196612
  5.5 8.0 %copy-start.5 = (bf16[64,512]{1,0:T(8,128)(2,1)S(1)}, bf16[64,512]{1,0:T(8,128)(2,1)}, u32[]{:S(2)}) copy-start(bf16[64,512]{1,0:T(8,128)(2,1)} %param.18) | copy-start | bytes 196612
  5.5 8.1 %copy-start.6 = (bf16[64,512]{1,0:T(8,128)(2,1)S(1)}, bf16[64,512]{1,0:T(8,128)(2,1)}, u32[]{:S(2)}) copy-start(bf16[64,512]{1,0:T(8,128)(2,1)} %param.19) | copy-start | bytes 196612
  10.9 3.6 %copy-start.2 = (bf16[128,2816]{1,0:T(8,128)(2,1)S(1)}, bf16[128,2816]{1,0:T(8,128)(2,1)}, u32[]{:S(2)}) copy-start(bf16[128,2816]{1,0:T(8,128)(2,1)} %param.28) | copy-start | bytes 2162692
  16.3 2.8 %copy-start.9 = (f32[8,8,8]{2,1,0:T(8,128)S(1)}, f32[8,8,8]{2,1,0:T(8,128)}, u32[]{:S(2)}) copy-start(f32[8,8,8]{2,1,0:T(8,128)} %get-tuple-element.23) | copy-start | bytes 6148
  16.4 2.9 %copy-start.1 = (f32[1,64,8,64]{3,2,1,0:T(8,128)S(1)}, f32[1,64,8,64]{3,2,1,0:T(8,128)}, u32[]{:S(2)}) copy-start(f32[1,64,8,64]{3,2,1,0:T(8,128)} %get-tuple-element.19) | copy-start | bytes 393220

commit v2 on v1

--- a/solution.py
+++ b/solution.py
@@ -107,7 +107,21 @@
         copy.wait()
 
 
-def chain_kernel(n, joined, entering, held, carried, send, recv, send_back, recv_back):
+def chain_kernel(
+    n,
+    joined,
+    weights,
+    entering,
+    spread,
+    held,
+    carried,
+    send,
+    recv,
+    send_back,
+    recv_back,
+    send_weights,
+    recv_weights,
+):
     me = lax.axis_index("sp")
     peers = [lax.rem(me + k, n) for k in range(1, n)]
     greet([{"sp": p} for p in peers])
@@ -120,6 +134,13 @@
     held[me] = joined[me]
     for copy in copies:
         copy.wait()
+    moves = [
+        remote(weights.at[p], spread.at[me], send_weights.at[k], recv_weights.at[k], {"sp": p})
+        for k, p in enumerate(peers)
+    ]
+    for copy in moves:
+        copy.start()
+    spread[me] = weights[me]
     size = entering.shape[1]
     back = me // (n // 2)
     state = jnp.zeros((size, size), F32)
@@ -143,7 +164,7 @@
     for copy in copies:
         copy.start()
     entering[me] = carried[me]
-    for copy in copies:
+    for copy in copies + moves:
         copy.wait()
 
 
@@ -448,12 +469,14 @@
 
     depth = perceptron_valve_factors.shape[0]
     units = perceptron_valve_factors.shape[1] // n
+    owners = 2 * heads == n
+    shrink = perceptron_shrink_factors.reshape(n, units, depth)
     weights = jnp.stack(
         [
             perceptron_valve_factors.T.reshape(n, units, depth),
             perceptron_widen_factors.T.reshape(n, units, depth),
-            perceptron_shrink_factors.reshape(n, units, depth),
-        ],
+        ]
+        + ([] if owners else [shrink]),
         1,
     )
     readings, joined, spread = pl.pallas_call(
@@ -470,22 +493,23 @@
         compiler_params=params(0),
     )(pack, vpad, weights)
 
-    if 2 * heads == n:
-        entering = pl.pallas_call(
+    if owners:
+        entering, narrow = pl.pallas_call(
             functools.partial(chain_kernel, n),
             name="chain",
-            out_shape=sds((n, size, size), BF),
-            in_specs=[VMEM],
-            out_specs=VMEM,
+            out_shape=(sds((n, size, size), BF), sds(shrink.shape, BF)),
+            in_specs=[VMEM] * 2,
+            out_specs=(VMEM,) * 2,
             scratch_shapes=[
                 pltpu.VMEM((n, size, 2 * size), BF),
                 pltpu.VMEM((n, size, size), BF),
             ]
-            + [dma((n - 1,))] * 4,
+            + [dma((n - 1,))] * 6,
             compiler_params=params(1),
-        )(joined)
+        )(joined, shrink)
     else:
         entering = chain_gathered(joined, n, heads, size)
+        narrow = spread[:, 2]
 
     residual = lax.dynamic_slice_in_dim(
         skip_stream_entering, lax.axis_index("tp") * share, share, 0
@@ -524,7 +548,7 @@
     tokens = gathered.reshape(-1, model)
     gate = spread[:, 0].transpose(0, 2, 1).reshape(model, units)
     up = spread[:, 1].transpose(0, 2, 1).reshape(model, units)
-    down = spread[:, 2].transpose(1, 0, 2).reshape(units, model)
+    down = narrow.transpose(1, 0, 2).reshape(units, model)
     inner = (
         jax.nn.silu(jnp.dot(tokens, gate, preferred_element_type=F32))
         * jnp.dot(tokens, up, preferred_element_type=F32)

time: 188 us -> 192 us (1.021)
  Pallas kernels: 152 us -> 158 us
    pallas_call x1, Pallas kernels: 26.9 us -> 33.4 us  [shards(): pl.pallas_call(functools.partial(chain_kernel, n), name='chain', out_shap...]
where the time goes in v2:
time: 192 us
  Pallas kernels  158 us (82%)
  local copies, waits for them, and re-layouts  13.1 us (7%)
  matrix products  10.7 us (6%)
  other arithmetic  9.73 us (5%)
    pallas_call x1, Pallas kernels, shards(): pl.pallas_call(functools.partial(recur_kernel, n), name='recur', out_shap...  54.5 us
    pallas_call x1, Pallas kernels, shards(): pl.pallas_call(functools.partial(gather_kernel, n1, n2, n_tp), name='gath...  35.8 us
    pallas_call x1, Pallas kernels, shards(): pl.pallas_call(functools.partial(scatter_kernel, n1, n2, n_tp), name='sca...  34.1 us
    pallas_call x1, Pallas kernels, shards(): pl.pallas_call(functools.partial(chain_kernel, n), name='chain', out_shap...  33.4 us
    mul x2, other arithmetic, shards(): jnp.sum(query * (written[0] + written[1]) * split(present_reward_factors)...  6.93 us
    dot_general x1, matrix products, shards(): terms = jnp.dot(inner, down, preferred_element_type=F32).astype(BF)  6.89 us

profile of v2, /device:TPU:0, one launch (start us, length us, event | category | flops | bytes accessed | tf_op | source)
XLA Modules:
  0.0 191.6 jit_solution(7664712622789358003)
XLA Ops:
  0.0 0.8 mul.49
  0.8 0.8 copy.34
  1.6 0.7 constant_dynamic-slice_fusion.residual
  2.3 1.0 reshape.80
  3.4 0.6 broadcast_add_fusion
  4.4 0.2 fusion.20
  5.0 0.2 copy-done.8
  5.5 5.4 %fusion = f32[64,8,64]{2,1,0:T(8,128)S(1)} fusion(f32[64,8,64]{2,1,0:T(8,128)S(1)} %reshape.82, f32[8,64]{1,0:T(8,128)S(1)} %mul.49, f32[2,64,8,64]{3,2,1,0:T(8,128)S(1)} %broadcast_multiply_fusion), kind=kOutput, calls=%fused_computation | output fusion | flops 98879 | bytes 526336 | tf_op jit(solution)/shard_map/mul | solution.py:466
  11.0 1.6 convert_multiply_fusion.bonus
  12.6 0.7 slice_bitcast_fusion.2
  13.8 0.7 pad_bitcast_fusion.vpad
  14.5 0.3 copy.39
  14.8 1.5 copy.40
  16.3 1.2 pad_maximum_fusion.weights
  17.9 0.4 copy.63
  18.3 1.8 copy.41.pack
  20.1 54.5 %recur.1 = (f32[2,8,64,128]{3,2,1,0:T(8,128)}, bf16[16,64,128]{2,1,0:T(8,128)(2,1)}, bf16[16,2,176,128]{3,2,1,0:T(8,128)(2,1)}) custom-call(f32[8,8,64,64]{3,2,1,0:T(8,128)} %copy.41.pack, f32[8,64,128]{2,1,0:T(8,128)} %pad_bitcast_fusion.vpad, bf16[16,2,176,128]{3,2,1,0:T(8,128)(2,1)} %pad_maximum_fusion.weights), custom_call_target="tpu_custom_call" | custom-call | tf_op jit(solution)/shard_map/recur/pallas_call | solution.py:482
  74.6 33.4 %chain.1 = (bf16[16,64,64]{2,1,0:T(8,128)(2,1)}, bf16[16,176,128]{2,1,0:T(8,128)(2,1)}) custom-call(bf16[16,64,128]{2,1,0:T(8,128)(2,1)} %get-tuple-element.13.joined, bf16[16,176,128]{2,1,0:T(8,128)(2,1)} %bitcast.79), custom_call_target="tpu_custom_call" | custom-call | tf_op jit(solution)/shard_map/chain/pallas_call | solution.py:497
  108.0 1.4 slice_bitcast_fusion.1
  109.5 35.8 %gather.1 = (bf16[2,4,4,32,2048]{4,3,2,1,0:T(8,128)(2,1)}, bf16[32,2048]{1,0:T(8,128)(2,1)}) custom-call(f32[2,8,64,128]{3,2,1,0:T(8,128)} %get-tuple-element.12.readings, bf16[16,64,64]{2,1,0:T(8,128)(2,1)} %get-tuple-element.14.entering, f32[64,512]{1,0:T(8,128)} %convert_multiply_fusion.bonus, bf16[64,512]{1,0:T(8,128)(2,1)} %valve.1, f32[1,512]{1,0:T(1,128)} %bitcast.83, ...), custom_call_target="tpu_custom_call" | custom-call | tf_op jit(solution)/shard_map/gather/pallas_call | solution.py:517
  145.3 3.8 %fusion.8 = f32[1024,176]{0,1:T(8,128)S(1)} fusion(bf16[1024,2048]{1,0:T(8,128)(2,1)} %bitcast.84, bf16[16,22,8,128]{3,2,1,0:T(8,128)(2,1)S(1)} %get-tuple-element.19), kind=kOutput, calls=%fused_computation.11 | convolution fusion | flops 738197504 | bytes 5636096 | tf_op jit(solution)/shard_map/dot_general | solution.py:553
  149.1 6.9 %convolution_convert_fusion = bf16[1024,2048]{1,0:T(8,128)(2,1)} fusion(bf16[1024,2048]{1,0:T(8,128)(2,1)} %bitcast.85, bf16[16,22,8,128]{3,2,1,0:T(8,128)(2,1)S(1)} %get-tuple-element.20, f32[1024,176]{0,1:T(8,128)S(1)} %fusion.8, bf16[16,176,128]{2,1,0:T(8,128)(2,1)S(1)} %copy-done.10), kind=kOutput, calls=%fused_computation.1 | convolution fusion | flops 1479573504 | bytes 10551296 | tf_op jit(solution)/shard_map/dot_general | solution.py:556
  156.0 34.1 %scatter.1 = bf16[32,2048]{1,0:T(8,128)(2,1)} custom-call(bf16[2,4,4,32,2048]{4,3,2,1,0:T(8,128)(2,1)} %bitcast.67, bf16[32,2048]{1,0:T(8,128)(2,1)} %get-tuple-element.18.middle, f32[1,2048]{1,0:T(1,128)} %bitcast.81), custom_call_target="tpu_custom_call" | custom-call | tf_op jit(solution)/shard_map/scatter/pallas_call | solution.py:558
  190.0 1.6 copy.72
  (47 shorter events, 1.9 us)
Async XLA Ops:
  0.0 1.6 copy-start
  0.0 4.2 %copy-start.3 = (bf16[64,512]{1,0:T(8,128)(2,1)S(1)}, bf16[64,512]{1,0:T(8,128)(2,1)}, u32[]{:S(2)}) copy-start(bf16[64,512]{1,0:T(8,128)(2,1)} %param.17) | copy-start | bytes 196612
  0.0 4.3 %copy-start.7 = (bf16[2,64,512]{2,1,0:T(8,128)(2,1)S(1)}, bf16[2,64,512]{2,1,0:T(8,128)(2,1)}, u32[]{:S(2)}) copy-start(bf16[2,64,512]{2,1,0:T(8,128)(2,1)} %param.21) | copy-start | bytes 393220
  4.3 0.9 copy-start.8
  5.5 7.8 %copy-start.4 = (bf16[64,512]{1,0:T(8,128)(2,1)S(1)}, bf16[64,512]{1,0:T(8,128)(2,1)}, u32[]{:S(2)}) copy-start(bf16[64,512]{1,0:T(8,128)(2,1)} %param.17) | copy-start | bytes 196612
  5.5 8.0 %copy-start.5 = (bf16[64,512]{1,0:T(8,128)(2,1)S(1)}, bf16[64,512]{1,0:T(8,128)(2,1)}, u32[]{:S(2)}) copy-start(bf16[64,512]{1,0:T(8,128)(2,1)} %param.18) | copy-start | bytes 196612
  5.5 8.1 %copy-start.6 = (bf16[64,512]{1,0:T(8,128)(2,1)S(1)}, bf16[64,512]{1,0:T(8,128)(2,1)}, u32[]{:S(2)}) copy-start(bf16[64,512]{1,0:T(8,128)(2,1)} %param.19) | copy-start | bytes 196612
  10.9 3.6 %copy-start.2 = (bf16[128,2816]{1,0:T(8,128)(2,1)S(1)}, bf16[128,2816]{1,0:T(8,128)(2,1)}, u32[]{:S(2)}) copy-start(bf16[128,2816]{1,0:T(8,128)(2,1)} %param.28) | copy-start | bytes 2162692
  16.3 1.3 copy-start.9
  16.3 1.4 copy-start.1
  145.2 3.8 %copy-start.10 = (bf16[16,176,128]{2,1,0:T(8,128)(2,1)S(1)}, bf16[16,176,128]{2,1,0:T(8,128)(2,1)}, u32[]{:S(2)}) copy-start(bf16[16,176,128]{2,1,0:T(8,128)(2,1)} %get-tuple-element.17) | copy-start | bytes 2162692
